TPU v7x, 32 devices: a whole 2x2x4 slice. The times are simulated.
32 devices in a mesh: fs: 8 (over z, x), tp: 4 (over y, core).
Axes of the slice: x: 2, y: 2, z: 4, core: 2. Of those that a mesh axis runs over, the one named last changes fastest.
Arguments:
- x_late: bfloat16 [3072, 2048], P(('fs', 'tp')), may hold values from -6 to 6
- x_early: bfloat16 [3072, 2048], P(('fs', 'tp')), may hold values from -6 to 6
- cotangent: bfloat16 [3072, 2048], P(('fs', 'tp')), may hold values from -6 to 6
- up_weight: bfloat16 [2048, 4096], P('fs', 'tp'), may hold values from -0.125 to 0.125
- down_weight: bfloat16 [2048, 4096], P('fs', 'tp'), may hold values from -0.09375 to 0.09375
- up_grad_sum: float32 [2048, 4096], P('fs', 'tp'), may hold values from -24 to 24
- down_grad_sum: float32 [2048, 4096], P('fs', 'tp'), may hold values from -24 to 24
Outputs:
- output: bfloat16 [3072, 2048], P(('fs', 'tp'))
- input_grad: bfloat16 [3072, 2048], P(('fs', 'tp'))
- up_grad_new: float32 [2048, 4096], P('fs', 'tp')
- down_grad_new: float32 [2048, 4096], P('fs', 'tp')
All inputs are finite; a program needn't handle non-finite values.
Results may differ from a plain program's by a relative error of at most 0.0095.
Values may be sent and summed in bfloat16 or wider, within the bound.
A program may use at most 128 MiB of HBM per device.

v0:
```python
import jax
import jax.numpy as jnp
from jax import lax
from jax.sharding import PartitionSpec as P


def dot_last(left, right):
    return lax.dot_general(
        left, right, (((1,), (1,)), ((), ())), preferred_element_type=jnp.float32
    )


def dot_first(left, right):
    return lax.dot_general(
        left, right, (((0,), (0,)), ((), ())), preferred_element_type=jnp.float32
    )


def squared(pre_act):
    return jnp.square(jax.nn.relu(pre_act)).astype(jnp.bfloat16)


def hidden_grad(grad_act, pre_early):
    return (grad_act * 2.0 * jax.nn.relu(pre_early)).astype(jnp.bfloat16)


def on_device(x_late, x_early, cotangent, up_weight, down_weight, up_grad_sum, down_grad_sum):
    late_rows, early_rows, cot_rows = (
        lax.all_gather(x_late, "tp", axis=0, tiled=True),
        lax.all_gather(x_early, "tp", axis=0, tiled=True),
        lax.all_gather(cotangent, "tp", axis=0, tiled=True),
    )
    block_cols = up_weight.shape[1]
    up_full, down_full = (
        lax.all_gather(up_weight, "fs", axis=0, tiled=True),
        lax.all_gather(down_weight, "fs", axis=0, tiled=True),
    )
    pre_late = jnp.dot(late_rows, up_full, preferred_element_type=jnp.float32)
    pre_early = jnp.dot(early_rows, up_full, preferred_element_type=jnp.float32)
    act_late = squared(pre_late)
    grad_act = jnp.dot(cot_rows, down_full, preferred_element_type=jnp.float32)
    act_early = squared(pre_early)
    grad_pre = hidden_grad(grad_act, pre_early)
    output = lax.psum_scatter(
        dot_last(act_late, down_full).astype(jnp.bfloat16), "tp", scatter_dimension=0, tiled=True
    )
    input_grad = lax.psum_scatter(
        dot_last(grad_pre, up_full).astype(jnp.bfloat16), "tp", scatter_dimension=0, tiled=True
    )
    summed = lax.psum_scatter(
        jnp.concatenate([dot_first(early_rows, grad_pre), dot_first(cot_rows, act_early)], axis=1),
        "fs",
        scatter_dimension=0,
        tiled=True,
    )
    up_added = summed[:, :block_cols]
    down_added = summed[:, block_cols:]
    return (output, input_grad, up_grad_sum + up_added, down_grad_sum + down_added)


def solution(mesh):
    placed = (
        P(("fs", "tp"), None),
        P(("fs", "tp"), None),
        P(("fs", "tp"), None),
        P("fs", "tp"),
        P("fs", "tp"),
        P("fs", "tp"),
        P("fs", "tp"),
    )
    return jax.shard_map(
        on_device,
        mesh=mesh,
        in_specs=placed,
        out_specs=(P(("fs", "tp"), None), P(("fs", "tp"), None), P("fs", "tp"), P("fs", "tp")),
        check_vma=False,
    )
```

profile of v0, /device:TPU:8, one launch (start us, length us, event | category | flops | bytes accessed | tf_op | source)
XLA Modules:
  0.0 571.7 jit_solution(4345790779414526677)
XLA Ops:
  7.2 0.7 all-gather.14.cloned.1.call-update
  7.9 0.7 all-gather.8.cloned.1.call-update
  10.6 19.8 %all-gather.14.cloned.1.call-done = bf16[384,2048]{1,0:T(8,128)(2,1)} async-done(((bf16[96,2048]{1,0:T(8,128)(2,1)}), bf16[384,2048]{1,0:T(8,128)(2,1)}) %all-gather.14.cloned.1.call-update) | async-done | bytes 1572880 | tf_op jit(solution)/shard_map/all_gather | solution.py:30
  30.4 74.6 %all-gather.8.cloned.1.call-done = bf16[2048,1024]{1,0:T(8,128)(2,1)} async-done(((bf16[256,1024]{1,0:T(8,128)(2,1)}), bf16[2048,1024]{1,0:T(8,128)(2,1)}) %all-gather.8.cloned.1.call-update) | async-done | bytes 4194320 | tf_op jit(solution)/shard_map/all_gather | solution.py:35
  105.0 4.5 convolution_maximum_fusion
  109.5 15.6 %all-gather.12.cloned.1.call-done = bf16[384,2048]{1,0:T(8,128)(2,1)} async-done(((bf16[96,2048]{1,0:T(8,128)(2,1)}), bf16[384,2048]{1,0:T(8,128)(2,1)}) %all-gather.12.cloned.1.call-update) | async-done | bytes 1572880 | tf_op jit(solution)/shard_map/all_gather | solution.py:31
  125.1 74.5 %all-gather.10.cloned.1.call-done = bf16[2048,1024]{1,0:T(8,128)(2,1)} async-done(((bf16[256,1024]{1,0:T(8,128)(2,1)}), bf16[2048,1024]{1,0:T(8,128)(2,1)}) %all-gather.10.cloned.1.call-update) | async-done | bytes 4194320 | tf_op jit(solution)/shard_map/all_gather | solution.py:36
  199.6 4.5 multiply_convert_fusion.1
  204.0 0.9 copy-done.3
  204.9 2.4 convolution_bitcast_fusion.1
  207.3 2.4 convolution_bitcast_fusion
  209.7 6.3 %pad_maximum_fusion = f32[2048,2048]{0,1:T(8,128)} fusion(f32[2048,1024]{0,1:T(8,128)S(1)} %convolution_bitcast_fusion, f32[2048,1024]{0,1:T(8,128)S(1)} %convolution_bitcast_fusion.1), kind=kLoop, calls=%fused_computation | loop fusion | flops 4194304 | bytes 33554432 | tf_op jit(solution)/shard_map/concatenate | solution.py:51
  216.1 3.4 all-gather.6.cloned.1.call-done
  219.5 8.6 %convolution_convert_fusion.1 = bf16[384,2048]{1,0:T(8,128)(2,1)} fusion(bf16[2048,1024]{1,0:T(8,128)(2,1)} %all-gather.10.cloned.1.call-done, bf16[384,2048]{1,0:T(8,128)(2,1)} %all-gather.6.cloned.1.call-done, bf16[2048,1024]{1,0:T(8,128)(2,1)} %all-gather.8.cloned.1.call-done), kind=kOutput, calls=%fused_computation.4 | convolution fusion | flops 3223191552 | bytes 11534336 | tf_op jit(solution)/shard_map/dot_general | solution.py:8
  228.3 0.9 copy-done.4
  229.2 5.9 %convolution_convert_fusion = bf16[384,2048]{1,0:T(8,128)(2,1)} fusion(bf16[384,1024]{1,0:T(8,128)(2,1)S(1)} %copy-done.4, bf16[2048,1024]{1,0:T(8,128)(2,1)} %all-gather.8.cloned.1.call-done), kind=kOutput, calls=%fused_computation.3 | convolution fusion | flops 1611399168 | bytes 6553600 | tf_op jit(solution)/shard_map/dot_general | solution.py:8
  235.1 1.2 copy-done.2
  236.6 1.6 copy.11
  238.2 264.2 %reduce-scatter.8.cloned.1.call-done = f32[256,2048]{0,1:T(8,128)} async-done(((f32[2048,2048]{0,1:T(8,128)}), f32[256,2048]{0,1:T(8,128)}) %reduce-scatter.8.cloned.1.call-update) | async-done | bytes 2097168 | tf_op jit(solution)/shard_map/reduce_scatter | solution.py:50
  502.4 2.8 slice_add_fusion
  505.2 2.5 copy.13
  507.7 1.3 copy.14
  509.0 24.7 %reduce-scatter.4.cloned.1.call-done = bf16[96,2048]{1,0:T(8,128)(2,1)} async-done(((bf16[384,2048]{1,0:T(8,128)(2,1)}), bf16[96,2048]{1,0:T(8,128)(2,1)}) %reduce-scatter.4.cloned.1.call-update) | async-done | bytes 393232 | tf_op jit(solution)/shard_map/reduce_scatter | solution.py:44
  533.7 31.1 %reduce-scatter.6.cloned.1.call-done = bf16[96,2048]{1,0:T(8,128)(2,1)} async-done(((bf16[384,2048]{1,0:T(8,128)(2,1)}), bf16[96,2048]{1,0:T(8,128)(2,1)}) %reduce-scatter.6.cloned.1.call-update) | async-done | bytes 393232 | tf_op jit(solution)/shard_map/reduce_scatter | solution.py:47
  (22 shorter events, 2.6 us)
Async XLA Ops:
  7.2 23.2 %all-gather.14.cloned.1.call-start = ((), (), s32[]{:S(2)}) async-start(), calls=%async_computation.8 | async-start | bytes 1966080 | tf_op jit(solution)/shard_map/all_gather | solution.py:30
  7.9 97.1 %all-gather.8.cloned.1.call-start = ((), (), s32[]{:S(2)}) async-start(), calls=%async_computation.4 | async-start | bytes 4718592 | tf_op jit(solution)/shard_map/all_gather | solution.py:35
  8.6 116.4 %all-gather.12.cloned.1.call-start = ((), (), s32[]{:S(2)}) async-start(), calls=%async_computation.7 | async-start | bytes 1966080 | tf_op jit(solution)/shard_map/all_gather | solution.py:31
  9.4 190.2 %all-gather.10.cloned.1.call-start = ((), (), s32[]{:S(2)}) async-start(), calls=%async_computation.5 | async-start | bytes 4718592 | tf_op jit(solution)/shard_map/all_gather | solution.py:36
  10.0 209.5 %all-gather.6.cloned.1.call-start = ((), (), s32[]{:S(2)}) async-start(), calls=%async_computation.3 | async-start | bytes 1966080 | tf_op jit(solution)/shard_map/all_gather | solution.py:29
  10.5 491.9 %reduce-scatter.8.cloned.1.call-start = ((), (), s32[]{:S(2)}) async-start(), calls=%async_computation.10 | async-start | bytes 18874368 | tf_op jit(solution)/shard_map/reduce_scatter | solution.py:50
  109.5 95.5 %copy-start = (bf16[384,2048]{1,0:T(8,128)(2,1)S(1)}, bf16[384,2048]{1,0:T(8,128)(2,1)}, u32[]{:S(2)}) copy-start(bf16[384,2048]{1,0:T(8,128)(2,1)} %all-gather.14.cloned.1.call-done) | copy-start | bytes 4718596
  204.0 0.9 copy-start.3
  204.9 2.4 copy-start.1
  216.1 317.6 %reduce-scatter.4.cloned.1.call-start = ((), (), s32[]{:S(2)}) async-start(), calls=%async_computation.6 | async-start | bytes 1966080 | tf_op jit(solution)/shard_map/reduce_scatter | solution.py:44
  228.1 1.1 copy-start.4
  228.1 336.8 %reduce-scatter.6.cloned.1.call-start = ((), (), s32[]{:S(2)}) async-start(), calls=%async_computation.9 | async-start | bytes 1966080 | tf_op jit(solution)/shard_map/reduce_scatter | solution.py:47
  235.1 1.2 copy-start.2
Sparse Core Ops, SparseCore 0:
  9.5 20.7 all-gather.13
  32.5 72.4 all-gather.7
  106.6 18.4 all-gather.11
  127.0 72.4 all-gather.9
  201.0 18.4 all-gather.5
  223.1 279.2 reduce-scatter.7
  505.5 28.1 reduce-scatter.3
  536.8 27.9 reduce-scatter.5
where the time goes:
time: 574 us; the launch traced here: 572 us
  waiting for transfers between devices  511 us (89%)
  matrix products  28.1 us (5%)
  between operations  14.2 us (2%)
  other arithmetic  9.09 us (2%)
  local copies, waits for them, and re-layouts  8.7 us (2%)
    reduce_scatter x1, waiting for transfers between devices, on_device(): lax.psum_scatter(jnp.concatenate([dot_first(early_rows, grad_pre), dot_fi...  264 us
    all_gather x1, waiting for transfers between devices, on_device(): lax.all_gather(up_weight, 'fs', axis=0, tiled=True)  74.6 us
    all_gather x1, waiting for transfers between devices, on_device(): lax.all_gather(down_weight, 'fs', axis=0, tiled=True)  74.5 us
    reduce_scatter x1, waiting for transfers between devices, on_device(): lax.psum_scatter(dot_last(grad_pre, up_full).astype(jnp.bfloat16), 'tp',...  31.1 us
    reduce_scatter x1, waiting for transfers between devices, on_device(): lax.psum_scatter(dot_last(act_late, down_full).astype(jnp.bfloat16), 'tp'...  24.7 us
    all_gather x1, waiting for transfers between devices, on_device(): lax.all_gather(x_early, 'tp', axis=0, tiled=True)  19.8 us
    all_gather x1, waiting for transfers between devices, on_device(): lax.all_gather(cotangent, 'tp', axis=0, tiled=True)  15.6 us
    dot_general x2, matrix products, dot_last(): lax.dot_general(left, right, (((1,), (1,)), ((), ())), preferred_element_...  14.4 us
  transfers between devices with their start and end apart: 8, of which 8 were waited for; matrix products, arithmetic and copies ran while one was open for 8% of the time, Pallas kernels for 0%

commit v1 on v0

v1 whole, which is shorter than its diff:
```python
import functools

import jax
import jax.numpy as jnp
from jax import lax
from jax.experimental import pallas as pl
from jax.experimental.pallas import tpu as pltpu
from jax.sharding import PartitionSpec as P


MESH = pl.DeviceIdType.MESH
ANY = pl.BlockSpec(memory_space=pl.ANY)
VMEM = pl.BlockSpec(memory_space=pltpu.VMEM)


def dot_last(left, right):
    return lax.dot_general(
        left, right, (((1,), (1,)), ((), ())), preferred_element_type=jnp.float32
    )


def dot_first(left, right):
    return lax.dot_general(
        left, right, (((0,), (0,)), ((), ())), preferred_element_type=jnp.float32
    )


def squared(pre_act):
    return jnp.square(jax.nn.relu(pre_act)).astype(jnp.bfloat16)


def hidden_grad(grad_act, pre_early):
    return (grad_act * 2.0 * jax.nn.relu(pre_early)).astype(jnp.bfloat16)


def flip(value, bit):
    return value + bit - 2 * bit * ((value // bit) % 2)


def remote(src, dst, send, recv, fs, tp):
    return pltpu.make_async_remote_copy(
        src_ref=src, dst_ref=dst, send_sem=send, recv_sem=recv,
        device_id={"fs": fs, "tp": tp}, device_id_type=MESH,
    )


def greet(peers):
    barrier = pltpu.get_barrier_semaphore()
    for fs, tp in peers:
        pl.semaphore_signal(barrier, inc=1, device_id={"fs": fs, "tp": tp}, device_id_type=MESH)
    pl.semaphore_wait(barrier, len(peers))


def gather_kernel(n_fo, n_tp, *refs):
    tokens, weights = refs[0:3], refs[3:5]
    all_tokens, all_weights = refs[5:8], refs[8:10]
    local, t_send, t_recv, x_send, x_recv, z_send, z_recv = refs[10:]
    fs, tp = lax.axis_index("fs"), lax.axis_index("tp")
    fo, fi = fs // 2, fs % 2
    pair = fo * 2 + 1 - fi
    half = weights[0].shape[1] // 2
    dims = n_tp.bit_length()

    def placed(mask):
        at_fi, at_tp = (1 - fi if mask & 1 else fi), tp
        for dim in range(1, dims):
            if (mask >> dim) & 1:
                at_tp = flip(at_tp, n_tp >> dim)
        return at_fi, at_tp

    def token(a, dim, mask):
        to_fi, to_tp = placed(1 << dim)
        slot = placed(mask)
        dst = all_tokens[a].at[slot[0], slot[1]]
        sem = mask + (1 << dim)
        return remote(tokens[a] if mask == 0 else dst, dst, t_send.at[a, sem], t_recv.at[a, sem],
                      fo * 2 + to_fi, to_tp)

    def columns(w, which):
        return weights[w].at[:, pl.ds(pl.multiple_of(which * half, half), half)]

    def across(w):
        return remote(columns(w, 1 - fi), all_weights[w].at[fs], x_send.at[w], x_recv.at[w], pair, tp)

    def along(w, step, part):
        dst = all_weights[w].at[pair if part else fs]
        return remote(dst if part else columns(w, fi), dst, z_send.at[w, step - 1, part],
                      z_recv.at[w, step - 1, part], ((fo + step) % n_fo) * 2 + fi, tp)

    peers = []
    for dim in range(dims):
        to_fi, to_tp = placed(1 << dim)
        peers.append((fo * 2 + to_fi, to_tp))
    for step in range(1, n_fo):
        peers.append((((fo + step) % n_fo) * 2 + fi, tp))
    greet(peers)

    for a in range(3):
        token(a, 0, 0).start()
        if a < 2:
            across(a).start()
    for w in range(2):
        for step in range(1, n_fo):
            along(w, step, 0).start()
    for a in range(3):
        for dim in range(1, dims):
            token(a, dim, 0).start()
    own = [pltpu.make_async_copy(tokens[a], all_tokens[a].at[fi, tp], local.at[a]) for a in range(3)]
    own += [pltpu.make_async_copy(columns(w, fi), all_weights[w].at[fs], local.at[3 + w]) for w in range(2)]
    for copy in own:
        copy.start()

    for dim in range(dims):
        for a in range(3):
            for mask in range(1 << dim):
                token(a, dim, mask).wait_recv()
                for later in range(dim + 1, dims):
                    token(a, later, mask + (1 << dim)).start()
            if dim == 0 and a < 2:
                across(a).wait_recv()
                for step in range(1, n_fo):
                    along(a, step, 1).start()
    for w in range(2):
        across(w).wait_send()
        for step in range(1, n_fo):
            for part in range(2):
                along(w, step, part).wait()
    for dim in range(dims):
        for a in range(3):
            for mask in range(1 << dim):
                token(a, dim, mask).wait_send()
    for copy in own:
        copy.wait()


def gather(n_fo, n_tp, tokens, weights):
    rows, width = tokens[0].shape
    w_rows, cols = weights[0].shape
    masks = 2 * n_tp
    dma = pltpu.SemaphoreType.DMA
    return pl.pallas_call(
        functools.partial(gather_kernel, n_fo, n_tp),
        out_shape=[jax.ShapeDtypeStruct((2, n_tp, rows, width), jnp.bfloat16)] * 3
        + [jax.ShapeDtypeStruct((2 * n_fo, w_rows, cols // 2), jnp.bfloat16)] * 2,
        in_specs=[VMEM] * 5,
        out_specs=[ANY] * 5,
        scratch_shapes=[
            dma((5,)), dma((3, masks)), dma((3, masks)), dma((2,)), dma((2,)),
            dma((2, n_fo - 1, 2)), dma((2, n_fo - 1, 2)),
        ],
        compiler_params=pltpu.CompilerParams(collective_id=0, has_side_effects=True),
        name="gather",
    )(*tokens, *weights)


def reduce_kernel(n_fo, n_tp, *refs):
    partial, grads = refs[0:2], refs[2:4]
    summed, mine, other = refs[4:6], refs[6:8], refs[8:10]
    (landed, pair_sum, arrived, g_in, staged,
     c_send, c_recv, t_send, t_recv, z_send, z_recv, x_send, x_recv) = refs[10:]
    fs, tp = lax.axis_index("fs"), lax.axis_index("tp")
    fo, fi = fs // 2, fs % 2
    pair = fo * 2 + 1 - fi
    n_y = n_tp // 2
    y, core = tp // 2, tp % 2
    others = [(dx, dy) for dy in range(n_y) for dx in range(2) if (dx, dy) != (0, 0)]

    def spot(dx, dy):
        return (1 - fi if dx else fi), (y + dy) % n_y

    def near(a):
        return remote(partial[a].at[:, :, 1 - core], landed.at[a], c_send.at[a], c_recv.at[a],
                      fs, y * 2 + 1 - core)

    def far(a, k):
        at_fi, at_y = spot(*others[k])
        return remote(pair_sum.at[a, at_fi, at_y], arrived.at[a, k], t_send.at[a, k], t_recv.at[a, k],
                      fo * 2 + at_fi, at_y * 2 + core)

    def along(w, step):
        to_fo = (fo + step) % n_fo
        return remote(grads[w].at[to_fo], g_in.at[w, step - 1], z_send.at[w, step - 1],
                      z_recv.at[w, step - 1], to_fo * 2 + fi, tp)

    def across(w):
        return remote(staged.at[w], other[w], x_send.at[w], x_recv.at[w], pair, tp)

    peers = [(fs, y * 2 + 1 - core)]
    for dx, dy in others:
        at_fi, at_y = spot(dx, dy)
        peers.append((fo * 2 + at_fi, at_y * 2 + core))
    for step in range(1, n_fo):
        peers.append((((fo + step) % n_fo) * 2 + fi, tp))
    greet(peers)

    for a in range(2):
        near(a).start()
    for w in range(2):
        for step in range(1, n_fo):
            along(w, step).start()

    def joined(a, at_fi, at_y):
        return (partial[a][at_fi, at_y, core].astype(jnp.float32)
                + landed[a, at_fi, at_y].astype(jnp.float32))

    for a in range(2):
        near(a).wait_recv()
        for k in range(len(others)):
            at_fi, at_y = spot(*others[k])
            pair_sum[a, at_fi, at_y] = joined(a, at_fi, at_y).astype(jnp.bfloat16)
            far(a, k).start()

    def owned(w, which):
        total = grads[w][fo, which].astype(jnp.float32)
        for step in range(1, n_fo):
            total += g_in[w, step - 1, which].astype(jnp.float32)
        return total

    for w in range(2):
        for step in range(1, n_fo):
            along(w, step).wait_recv()
        staged[w] = owned(w, 1 - fi).astype(jnp.bfloat16)
        across(w).start()
        mine[w][...] = owned(w, fi)
    for a in range(2):
        total = joined(a, fi, y)
        for k in range(len(others)):
            far(a, k).wait_recv()
            total += arrived[a, k].astype(jnp.float32)
        summed[a][...] = total.astype(jnp.bfloat16)
    for w in range(2):
        across(w).wait()
        for step in range(1, n_fo):
            along(w, step).wait_send()
    for a in range(2):
        near(a).wait_send()
        for k in range(len(others)):
            far(a, k).wait_send()


def reduce(n_fo, n_tp, partial, grads):
    rows, width = partial[0].shape[-2:]
    w_rows, half = grads[0].shape[-2:]
    n_y = n_tp // 2
    others = 2 * n_y - 1
    dma = pltpu.SemaphoreType.DMA
    bf16, f32 = jnp.bfloat16, jnp.float32
    return pl.pallas_call(
        functools.partial(reduce_kernel, n_fo, n_tp),
        out_shape=[jax.ShapeDtypeStruct((rows, width), bf16)] * 2
        + [jax.ShapeDtypeStruct((w_rows, half), f32)] * 2
        + [jax.ShapeDtypeStruct((w_rows, half), bf16)] * 2,
        in_specs=[VMEM] * 4,
        out_specs=[VMEM] * 6,
        scratch_shapes=[
            pltpu.VMEM((2, 2, n_y, rows, width), bf16),
            pltpu.VMEM((2, 2, n_y, rows, width), bf16),
            pltpu.VMEM((2, others, rows, width), bf16),
            pltpu.VMEM((2, n_fo - 1, 2, w_rows, half), bf16),
            pltpu.VMEM((2, w_rows, half), bf16),
            dma((2,)), dma((2,)), dma((2, others)), dma((2, others)),
            dma((2, n_fo - 1)), dma((2, n_fo - 1)), dma((2,)), dma((2,)),
        ],
        compiler_params=pltpu.CompilerParams(collective_id=1, has_side_effects=True),
        name="reduce",
    )(*partial, *grads)


def on_device(n_fo, n_tp, x_late, x_early, cotangent, up_weight, down_weight, up_grad_sum, down_grad_sum):
    rows, width = x_late.shape
    w_rows, cols = up_weight.shape
    half = cols // 2
    late, early, cot, up, down = gather(n_fo, n_tp, (x_late, x_early, cotangent), (up_weight, down_weight))
    late, early, cot = (a.reshape(-1, width) for a in (late, early, cot))
    up, down = (a.reshape(-1, half) for a in (up, down))
    pre_late = jnp.dot(late, up, preferred_element_type=jnp.float32)
    pre_early = jnp.dot(early, up, preferred_element_type=jnp.float32)
    act_late = squared(pre_late)
    grad_act = jnp.dot(cot, down, preferred_element_type=jnp.float32)
    act_early = squared(pre_early)
    grad_pre = hidden_grad(grad_act, pre_early)
    partial = [
        value.astype(jnp.bfloat16).reshape(2, n_tp // 2, 2, rows, width)
        for value in (dot_last(act_late, down), dot_last(grad_pre, up))
    ]
    grads = [
        value.astype(jnp.bfloat16).reshape(n_fo, 2, w_rows, half)
        for value in (dot_first(early, grad_pre), dot_first(cot, act_early))
    ]
    output, input_grad, up_mine, down_mine, up_other, down_other = reduce(n_fo, n_tp, partial, grads)
    low = lax.axis_index("fs") % 2 == 0

    def added(total, mine, other):
        other = other.astype(jnp.float32)
        return total + jnp.concatenate([jnp.where(low, mine, other), jnp.where(low, other, mine)], axis=1)

    return (output, input_grad, added(up_grad_sum, up_mine, up_other), added(down_grad_sum, down_mine, down_other))


def solution(mesh):
    rows, both = P(("fs", "tp"), None), P("fs", "tp")
    return jax.shard_map(
        functools.partial(on_device, mesh.shape["fs"] // 2, mesh.shape["tp"]),
        mesh=mesh,
        in_specs=(rows, rows, rows, both, both, both, both),
        out_specs=(rows, rows, both, both),
        check_vma=False,
    )
```

time: 574 us -> 232 us (0.40)
  waiting for transfers between devices: 511 us -> 0 us
  Pallas kernels: 0 us -> 201 us
  between operations: 14.2 us -> 0.74 us
  local copies, waits for them, and re-layouts: 8.7 us -> 1.94 us
    reduce_scatter x3 -> x0, waiting for transfers between devices: 320 us -> none  [the longest x1 264 us: on_device(): lax.psum_scatter(jnp.concatenate([dot_first(early_rows, grad_pre), dot_fi...]
    pallas_call x0 -> x2, Pallas kernels: none -> 201 us  [the longest x1 105 us: reduce(): pl.pallas_call(functools.partial(reduce_kernel, n_fo, n_tp), out_shape=[j...]
    all_gather x5 -> x0, waiting for transfers between devices: 188 us -> none  [the longest x1 74.6 us: on_device(): lax.all_gather(up_weight, 'fs', axis=0, tiled=True)]
    unnamed x14 -> x18, local copies, waits for them, and re-layouts: 8.7 us -> 1.94 us
    concatenate x1 -> x0, other arithmetic: 6.31 us -> none  [on_device(): jnp.concatenate([dot_first(early_rows, grad_pre), dot_first(cot_rows, act...]
  transfers between devices with their start and end apart: 8 -> 0, of which waited for: 8 -> 0; matrix products, arithmetic and copies ran while one was open for 8% -> 0% of each run, Pallas kernels for 0% -> 0%
where the time goes in v1:
time: 232 us; the launch traced here: 231 us
  Pallas kernels  201 us (87%)
  matrix products  23.6 us (10%)
  other arithmetic  3.95 us (2%)
    pallas_call x1, Pallas kernels, reduce(): pl.pallas_call(functools.partial(reduce_kernel, n_fo, n_tp), out_shape=[j...  105 us
    pallas_call x1, Pallas kernels, gather(): pl.pallas_call(functools.partial(gather_kernel, n_fo, n_tp), out_shape=[j...  96 us
    dot_general x2, matrix products, dot_last(): lax.dot_general(left, right, (((1,), (1,)), ((), ())), preferred_element_...  11.9 us
    dot_general x2, matrix products, dot_first(): lax.dot_general(left, right, (((0,), (0,)), ((), ())), preferred_element_...  6.42 us

profile of v1, /device:TPU:8, one launch (start us, length us, event | category | flops | bytes accessed | tf_op | source)
XLA Modules:
  0.0 231.3 jit_solution(1635581576977752053)
XLA Ops:
  0.6 96.0 %gather.1 = (bf16[2,4,96,2048]{3,2,1,0:T(8,128)(2,1)}, bf16[2,4,96,2048]{3,2,1,0:T(8,128)(2,1)}, bf16[2,4,96,2048]{3,2,1,0:T(8,128)(2,1)}, bf16[8,256,512]{2,1,0:T(8,128)(2,1)}, bf16[8,256,512]{2,1,0:T(8,128)(2,1)}) custom-call(bf16[96,2048]{1,0:T(8,128)(2,1)} %refs_0_.1, bf16[96,2048]{1,0:T(8,128)(2,1)} %refs_1_.1, bf16[96,2048]{1,0:T(8,128)(2,1)} %refs_2_.1, ...), custom_call_target="tpu_custom_call" | custom-call | tf_op jit(solution)/shard_map/gather/pallas_call | solution.py:141
  96.6 0.0 copy-start.4
  96.6 8.3 %convolution_convert_fusion.1 = bf16[768,2048]{1,0:T(8,128)(2,1)} fusion(bf16[2048,512]{1,0:T(8,128)(2,1)} %bitcast.33, bf16[768,2048]{1,0:T(8,128)(2,1)} %bitcast.29, bf16[2048,512]{1,0:T(8,128)(2,1)} %bitcast.30), kind=kOutput, calls=%fused_computation.1 | convolution fusion | flops 3223977984 | bytes 10485760 | tf_op jit(solution)/shard_map/dot_general | solution.py:17
  105.0 0.0 copy-done.4
  105.0 3.5 %convolution_maximum_fusion = f32[768,512]{1,0:T(8,128)S(1)} fusion(bf16[768,2048]{1,0:T(8,128)(2,1)S(1)} %bitcast.25, bf16[2048,512]{1,0:T(8,128)(2,1)} %bitcast.31), kind=kOutput, calls=%fused_computation.7 | convolution fusion | flops 1611005952 | bytes 6815744 | tf_op jit(solution)/shard_map/dot_general | solution.py:277
  108.5 0.0 copy-done.5
  108.5 0.0 copy-done.7
  108.6 1.8 multiply_convert_fusion.1
  110.3 3.2 %convolution_convert_fusion.2 = bf16[2048,512]{1,0:T(8,128)(2,1)} fusion(bf16[768,2048]{1,0:T(8,128)(2,1)S(1)} %bitcast.28, f32[768,512]{1,0:T(8,128)S(1)} %convolution_maximum_fusion), kind=kOutput, calls=%fused_computation.2 | convolution fusion | flops 1612447744 | bytes 6815744 | tf_op jit(solution)/shard_map/dot_general | solution.py:23
  113.6 3.2 %convolution_convert_fusion.3 = bf16[2048,512]{1,0:T(8,128)(2,1)} fusion(bf16[768,2048]{1,0:T(8,128)(2,1)S(1)} %bitcast.26, bf16[768,512]{1,0:T(8,128)(2,1)S(1)} %multiply_convert_fusion.1), kind=kOutput, calls=%fused_computation.3 | convolution fusion | flops 1611661312 | bytes 6029312 | tf_op jit(solution)/shard_map/dot_general | solution.py:23
  116.8 0.0 copy-done.6
  116.8 3.5 %convolution_convert_fusion = bf16[768,2048]{1,0:T(8,128)(2,1)} fusion(bf16[768,512]{1,0:T(8,128)(2,1)S(1)} %multiply_convert_fusion.1, bf16[2048,512]{1,0:T(8,128)(2,1)S(1)} %bitcast.32), kind=kOutput, calls=%fused_computation | convolution fusion | flops 1612185600 | bytes 6029312 | tf_op jit(solution)/shard_map/dot_general | solution.py:17
  120.3 105.1 %reduce.1 = (bf16[96,2048]{1,0:T(8,128)(2,1)}, bf16[96,2048]{1,0:T(8,128)(2,1)}, f32[256,512]{1,0:T(8,128)}, f32[256,512]{1,0:T(8,128)}, bf16[256,512]{1,0:T(8,128)(2,1)}, /*index=5*/bf16[256,512]{1,0:T(8,128)(2,1)}) custom-call(bf16[2,2,2,96,2048]{4,3,2,1,0:T(8,128)(2,1)} %bitcast.21, bf16[2,2,2,96,2048]{4,3,2,1,0:T(8,128)(2,1)} %bitcast.22, ...), custom_call_target="tpu_custom_call" | custom-call | tf_op jit(solution)/shard_map/reduce/pallas_call | solution.py:248
  225.4 0.0 copy-start
  225.4 1.7 convert_select_fusion.1
  227.1 0.0 copy-start.1
  227.1 0.0 copy-done
  227.1 1.1 maximum_add_fusion.1
  228.2 0.4 copy-done.1
  228.7 1.1 maximum_add_fusion
  229.8 0.0 copy-done.3
  229.8 0.7 copy.13
  230.5 0.0 copy-done.2
  230.5 0.7 copy.14
  (5 shorter events, 0.0 us)
Async XLA Ops:
  96.6 8.4 %copy-start.4 = (bf16[2,4,96,2048]{3,2,1,0:T(8,128)(2,1)S(1)}, bf16[2,4,96,2048]{3,2,1,0:T(8,128)(2,1)}, u32[]{:S(2)}) copy-start(bf16[2,4,96,2048]{3,2,1,0:T(8,128)(2,1)} %get-tuple-element.19) | copy-start | bytes 9437188
  105.0 3.5 %copy-start.5 = (bf16[2,4,96,2048]{3,2,1,0:T(8,128)(2,1)S(1)}, bf16[2,4,96,2048]{3,2,1,0:T(8,128)(2,1)}, u32[]{:S(2)}) copy-start(bf16[2,4,96,2048]{3,2,1,0:T(8,128)(2,1)} %get-tuple-element.18) | copy-start | bytes 9437188
  105.0 3.6 %copy-start.7 = (bf16[8,256,512]{2,1,0:T(8,128)(2,1)S(1)}, bf16[8,256,512]{2,1,0:T(8,128)(2,1)}, u32[]{:S(2)}) copy-start(bf16[8,256,512]{2,1,0:T(8,128)(2,1)} %get-tuple-element.17) | copy-start | bytes 6291460
  113.6 3.2 %copy-start.6 = (bf16[8,256,512]{2,1,0:T(8,128)(2,1)S(1)}, bf16[8,256,512]{2,1,0:T(8,128)(2,1)}, u32[]{:S(2)}) copy-start(bf16[8,256,512]{2,1,0:T(8,128)(2,1)} %get-tuple-element.16) | copy-start | bytes 6291460
  225.4 1.7 copy-start
  227.1 1.6 copy-start.1
  228.7 1.1 copy-start.3
  228.7 1.9 copy-start.2

commit v2 on v1

--- a/solution.py
+++ b/solution.py
@@ -82,26 +82,50 @@
     def across(w):
         return remote(columns(w, 1 - fi), all_weights[w].at[fs], x_send.at[w], x_recv.at[w], pair, tp)
 
-    def along(w, step, part):
-        dst = all_weights[w].at[pair if part else fs]
-        return remote(dst if part else columns(w, fi), dst, z_send.at[w, step - 1, part],
-                      z_recv.at[w, step - 1, part], ((fo + step) % n_fo) * 2 + fi, tp)
+    def along(w, source, part, way):
+        dst = all_weights[w].at[source * 2 + (1 - fi if part else fi)]
+        return dst, z_send.at[way, w, source, part], z_recv.at[w, source, part], ((fo + 1 - 2 * way) % n_fo) * 2 + fi
+
+    def relay(w, source, part, way):
+        dst, send, recv, to = along(w, source, part, way)
+        return remote(dst, dst, send, recv, to, tp)
+
+    def begin(w, way):
+        dst, send, recv, to = along(w, fo, 0, way)
+        return remote(columns(w, fi), dst, send, recv, to, tp)
+
+    def open_way(way):
+        return fo < n_fo - 1 if way == 0 else fo > 0
+
+    def take(w, part, distance):
+        for way in range(2):
+            source = fo - distance if way == 0 else fo + distance
+
+            @pl.when((source >= 0) & (source < n_fo))
+            def _():
+                relay(w, source, part, way).wait_recv()
+
+                @pl.when(open_way(way))
+                def _():
+                    relay(w, source, part, way).start()
 
     peers = []
     for dim in range(dims):
         to_fi, to_tp = placed(1 << dim)
         peers.append((fo * 2 + to_fi, to_tp))
-    for step in range(1, n_fo):
+    for step in (1, n_fo - 1):
         peers.append((((fo + step) % n_fo) * 2 + fi, tp))
     greet(peers)
 
+    for way in range(2):
+        @pl.when(open_way(way))
+        def _():
+            for w in range(2):
+                begin(w, way).start()
     for a in range(3):
         token(a, 0, 0).start()
         if a < 2:
             across(a).start()
-    for w in range(2):
-        for step in range(1, n_fo):
-            along(w, step, 0).start()
     for a in range(3):
         for dim in range(1, dims):
             token(a, dim, 0).start()
@@ -110,21 +134,53 @@
     for copy in own:
         copy.start()
 
-    for dim in range(dims):
-        for a in range(3):
-            for mask in range(1 << dim):
-                token(a, dim, mask).wait_recv()
-                for later in range(dim + 1, dims):
-                    token(a, later, mask + (1 << dim)).start()
-            if dim == 0 and a < 2:
-                across(a).wait_recv()
-                for step in range(1, n_fo):
-                    along(a, step, 1).start()
+    def passed(a, dim, mask):
+        token(a, dim, mask).wait_recv()
+        for later in range(dim + 1, dims):
+            token(a, later, mask + (1 << dim)).start()
+
+    def crossed(w):
+        across(w).wait_recv()
+        for way in range(2):
+            @pl.when(open_way(way))
+            def _():
+                relay(w, fo, 1, way).start()
+
+    take(0, 0, 1)
+    take(1, 0, 1)
+    passed(0, 0, 0)
+    crossed(0)
+    for distance in range(2, n_fo):
+        take(0, 0, distance)
+        take(1, 0, distance)
+        if distance == 2:
+            passed(1, 0, 0)
+            crossed(1)
+            take(0, 1, 1)
+            passed(2, 0, 0)
+    take(1, 1, 1)
+    for distance in range(2, n_fo - 1):
+        take(0, 1, distance)
+        take(1, 1, distance)
+    for dim in range(1, dims):
+        for mask in range(1 << dim):
+            for a in range(3):
+                passed(a, dim, mask)
     for w in range(2):
+        take(w, 1, n_fo - 1)
         across(w).wait_send()
-        for step in range(1, n_fo):
-            for part in range(2):
-                along(w, step, part).wait()
+        for way in range(2):
+            @pl.when(open_way(way))
+            def _():
+                begin(w, way).wait_send()
+                relay(w, fo, 1, way).wait_send()
+                for distance in range(1, n_fo):
+                    source = fo - distance if way == 0 else fo + distance
+
+                    @pl.when((source >= 0) & (source < n_fo))
+                    def _():
+                        for part in range(2):
+                            relay(w, source, part, way).wait_send()
     for dim in range(dims):
         for a in range(3):
             for mask in range(1 << dim):
@@ -146,7 +202,7 @@
         out_specs=[ANY] * 5,
         scratch_shapes=[
             dma((5,)), dma((3, masks)), dma((3, masks)), dma((2,)), dma((2,)),
-            dma((2, n_fo - 1, 2)), dma((2, n_fo - 1, 2)),
+            dma((2, 2, n_fo, 2)), dma((2, n_fo, 2)),
         ],
         compiler_params=pltpu.CompilerParams(collective_id=0, has_side_effects=True),
         name="gather",
@@ -177,10 +233,16 @@
         return remote(pair_sum.at[a, at_fi, at_y], arrived.at[a, k], t_send.at[a, k], t_recv.at[a, k],
                       fo * 2 + at_fi, at_y * 2 + core)
 
-    def along(w, step):
-        to_fo = (fo + step) % n_fo
-        return remote(grads[w].at[to_fo], g_in.at[w, step - 1], z_send.at[w, step - 1],
-                      z_recv.at[w, step - 1], to_fo * 2 + fi, tp)
+    def along(w, block, way, src):
+        return remote(src, g_in.at[way, w, block], z_send.at[way, w, block], z_recv.at[way, w, block],
+                      ((fo + 1 - 2 * way) % n_fo) * 2 + fi, tp)
+
+    def onward(way, distance, action):
+        block = fo + distance if way == 0 else fo - distance
+        first = fo == 0 if way == 0 else fo == n_fo - 1
+        inside = (block >= 0) & (block < n_fo)
+        for w in range(2):
+            action(w, block, first, inside)
 
     def across(w):
         return remote(staged.at[w], other[w], x_send.at[w], x_recv.at[w], pair, tp)
@@ -189,15 +251,20 @@
     for dx, dy in others:
         at_fi, at_y = spot(dx, dy)
         peers.append((fo * 2 + at_fi, at_y * 2 + core))
-    for step in range(1, n_fo):
+    for step in (1, n_fo - 1):
         peers.append((((fo + step) % n_fo) * 2 + fi, tp))
     greet(peers)
 
     for a in range(2):
         near(a).start()
-    for w in range(2):
-        for step in range(1, n_fo):
-            along(w, step).start()
+    for way in range(2):
+        def launch(w, block, first, inside):
+            @pl.when(first & inside)
+            def _():
+                along(w, block, way, grads[w].at[block]).start()
+
+        for distance in range(n_fo - 1, 0, -1):
+            onward(way, distance, launch)
 
     def joined(a, at_fi, at_y):
         return (partial[a][at_fi, at_y, core].astype(jnp.float32)
@@ -210,15 +277,38 @@
             pair_sum[a, at_fi, at_y] = joined(a, at_fi, at_y).astype(jnp.bfloat16)
             far(a, k).start()
 
+    for distance in range(n_fo - 2, 0, -1):
+        for way in range(2):
+            def carry(w, block, first, inside):
+                @pl.when(jnp.logical_not(first) & inside)
+                def _():
+                    held = g_in.at[way, w, block]
+                    along(w, block, way, held).wait_recv()
+                    for part in range(2):
+                        g_in[way, w, block, part] = (
+                            grads[w][block, part].astype(jnp.float32)
+                            + g_in[way, w, block, part].astype(jnp.float32)
+                        ).astype(jnp.bfloat16)
+                    along(w, block, way, held).start()
+
+            onward(way, distance, carry)
+
     def owned(w, which):
-        total = grads[w][fo, which].astype(jnp.float32)
-        for step in range(1, n_fo):
-            total += g_in[w, step - 1, which].astype(jnp.float32)
-        return total
+        return (grads[w][fo, which].astype(jnp.float32)
+                + g_in[0, w, fo, which].astype(jnp.float32)
+                + g_in[1, w, fo, which].astype(jnp.float32))
 
     for w in range(2):
-        for step in range(1, n_fo):
-            along(w, step).wait_recv()
+        for way in range(2):
+            first = fo == 0 if way == 0 else fo == n_fo - 1
+
+            @pl.when(first)
+            def _():
+                g_in[way, w, fo] = jnp.zeros(g_in.shape[3:], g_in.dtype)
+
+            @pl.when(jnp.logical_not(first))
+            def _():
+                along(w, fo, way, g_in.at[way, w, fo]).wait_recv()
         staged[w] = owned(w, 1 - fi).astype(jnp.bfloat16)
         across(w).start()
         mine[w][...] = owned(w, fi)
@@ -230,8 +320,14 @@
         summed[a][...] = total.astype(jnp.bfloat16)
     for w in range(2):
         across(w).wait()
-        for step in range(1, n_fo):
-            along(w, step).wait_send()
+    for way in range(2):
+        def finish(w, block, first, inside):
+            @pl.when(inside)
+            def _():
+                along(w, block, way, grads[w].at[block]).wait_send()
+
+        for distance in range(n_fo - 1, 0, -1):
+            onward(way, distance, finish)
     for a in range(2):
         near(a).wait_send()
         for k in range(len(others)):
@@ -256,10 +352,10 @@
             pltpu.VMEM((2, 2, n_y, rows, width), bf16),
             pltpu.VMEM((2, 2, n_y, rows, width), bf16),
             pltpu.VMEM((2, others, rows, width), bf16),
-            pltpu.VMEM((2, n_fo - 1, 2, w_rows, half), bf16),
+            pltpu.VMEM((2, 2, n_fo, 2, w_rows, half), bf16),
             pltpu.VMEM((2, w_rows, half), bf16),
             dma((2,)), dma((2,)), dma((2, others)), dma((2, others)),
-            dma((2, n_fo - 1)), dma((2, n_fo - 1)), dma((2,)), dma((2,)),
+            dma((2, 2, n_fo)), dma((2, 2, n_fo)), dma((2,)), dma((2,)),
         ],
         compiler_params=pltpu.CompilerParams(collective_id=1, has_side_effects=True),
         name="reduce",

time: 232 us -> 188 us (0.81)
  Pallas kernels: 201 us -> 156 us
    pallas_call x1, Pallas kernels: 96 us -> 71.6 us  [gather(): pl.pallas_call(functools.partial(gather_kernel, n_fo, n_tp), out_shape=[j...]
    pallas_call x1, Pallas kernels: 105 us -> 84.1 us  [reduce(): pl.pallas_call(functools.partial(reduce_kernel, n_fo, n_tp), out_shape=[j...]
where the time goes in v2:
time: 188 us; the launch traced here: 186 us
  Pallas kernels  156 us (83%)
  matrix products  23.6 us (13%)
  other arithmetic  3.95 us (2%)
  local copies, waits for them, and re-layouts  1.94 us (1%)
    pallas_call x1, Pallas kernels, reduce(): pl.pallas_call(functools.partial(reduce_kernel, n_fo, n_tp), out_shape=[j...  84.1 us
    pallas_call x1, Pallas kernels, gather(): pl.pallas_call(functools.partial(gather_kernel, n_fo, n_tp), out_shape=[j...  71.6 us
    dot_general x2, matrix products, dot_last(): lax.dot_general(left, right, (((1,), (1,)), ((), ())), preferred_element_...  11.9 us
    dot_general x2, matrix products, dot_first(): lax.dot_general(left, right, (((0,), (0,)), ((), ())), preferred_element_...  6.41 us

profile of v2, /device:TPU:8, one launch (start us, length us, event | category | flops | bytes accessed | tf_op | source)
XLA Modules:
  0.0 185.9 jit_solution(1494501199412738440)
XLA Ops:
  0.6 71.6 %gather.1 = (bf16[2,4,96,2048]{3,2,1,0:T(8,128)(2,1)}, bf16[2,4,96,2048]{3,2,1,0:T(8,128)(2,1)}, bf16[2,4,96,2048]{3,2,1,0:T(8,128)(2,1)}, bf16[8,256,512]{2,1,0:T(8,128)(2,1)}, bf16[8,256,512]{2,1,0:T(8,128)(2,1)}) custom-call(bf16[96,2048]{1,0:T(8,128)(2,1)} %refs_0_.1, bf16[96,2048]{1,0:T(8,128)(2,1)} %refs_1_.1, bf16[96,2048]{1,0:T(8,128)(2,1)} %refs_2_.1, ...), custom_call_target="tpu_custom_call" | custom-call | tf_op jit(solution)/shard_map/gather/pallas_call | solution.py:197
  72.3 0.0 copy-start.4
  72.3 8.4 %convolution_convert_fusion.1 = bf16[768,2048]{1,0:T(8,128)(2,1)} fusion(bf16[2048,512]{1,0:T(8,128)(2,1)} %bitcast.33, bf16[768,2048]{1,0:T(8,128)(2,1)} %bitcast.29, bf16[2048,512]{1,0:T(8,128)(2,1)} %bitcast.30), kind=kOutput, calls=%fused_computation.1 | convolution fusion | flops 3223977984 | bytes 10485760 | tf_op jit(solution)/shard_map/dot_general | solution.py:17
  80.6 0.0 copy-done.4
  80.6 3.5 %convolution_maximum_fusion = f32[768,512]{1,0:T(8,128)S(1)} fusion(bf16[768,2048]{1,0:T(8,128)(2,1)S(1)} %bitcast.25, bf16[2048,512]{1,0:T(8,128)(2,1)} %bitcast.31), kind=kOutput, calls=%fused_computation.7 | convolution fusion | flops 1611005952 | bytes 6815744 | tf_op jit(solution)/shard_map/dot_general | solution.py:373
  84.2 0.0 copy-done.5
  84.2 0.0 copy-done.7
  84.2 1.8 multiply_convert_fusion.1
  86.0 3.2 %convolution_convert_fusion.2 = bf16[2048,512]{1,0:T(8,128)(2,1)} fusion(bf16[768,2048]{1,0:T(8,128)(2,1)S(1)} %bitcast.28, f32[768,512]{1,0:T(8,128)S(1)} %convolution_maximum_fusion), kind=kOutput, calls=%fused_computation.2 | convolution fusion | flops 1612447744 | bytes 6815744 | tf_op jit(solution)/shard_map/dot_general | solution.py:23
  89.2 3.2 %convolution_convert_fusion.3 = bf16[2048,512]{1,0:T(8,128)(2,1)} fusion(bf16[768,2048]{1,0:T(8,128)(2,1)S(1)} %bitcast.26, bf16[768,512]{1,0:T(8,128)(2,1)S(1)} %multiply_convert_fusion.1), kind=kOutput, calls=%fused_computation.3 | convolution fusion | flops 1611661312 | bytes 6029312 | tf_op jit(solution)/shard_map/dot_general | solution.py:23
  92.4 0.0 copy-done.6
  92.4 3.5 %convolution_convert_fusion = bf16[768,2048]{1,0:T(8,128)(2,1)} fusion(bf16[768,512]{1,0:T(8,128)(2,1)S(1)} %multiply_convert_fusion.1, bf16[2048,512]{1,0:T(8,128)(2,1)S(1)} %bitcast.32), kind=kOutput, calls=%fused_computation | convolution fusion | flops 1612185600 | bytes 6029312 | tf_op jit(solution)/shard_map/dot_general | solution.py:17
  95.9 84.1 %reduce.1 = (bf16[96,2048]{1,0:T(8,128)(2,1)}, bf16[96,2048]{1,0:T(8,128)(2,1)}, f32[256,512]{1,0:T(8,128)}, f32[256,512]{1,0:T(8,128)}, bf16[256,512]{1,0:T(8,128)(2,1)}, /*index=5*/bf16[256,512]{1,0:T(8,128)(2,1)}) custom-call(bf16[2,2,2,96,2048]{4,3,2,1,0:T(8,128)(2,1)} %bitcast.21, bf16[2,2,2,96,2048]{4,3,2,1,0:T(8,128)(2,1)} %bitcast.22, ...), custom_call_target="tpu_custom_call" | custom-call | tf_op jit(solution)/shard_map/reduce/pallas_call | solution.py:344
  180.0 0.0 copy-start
  180.0 1.7 convert_select_fusion.1
  181.7 0.0 copy-start.1
  181.7 0.0 copy-done
  181.7 1.1 maximum_add_fusion.1
  182.9 0.4 copy-done.1
  183.3 1.1 maximum_add_fusion
  184.4 0.0 copy-done.3
  184.4 0.7 copy.13
  185.1 0.0 copy-done.2
  185.1 0.7 copy.14
  (5 shorter events, 0.0 us)
Async XLA Ops:
  72.3 8.4 %copy-start.4 = (bf16[2,4,96,2048]{3,2,1,0:T(8,128)(2,1)S(1)}, bf16[2,4,96,2048]{3,2,1,0:T(8,128)(2,1)}, u32[]{:S(2)}) copy-start(bf16[2,4,96,2048]{3,2,1,0:T(8,128)(2,1)} %get-tuple-element.19) | copy-start | bytes 9437188
  80.6 3.5 %copy-start.5 = (bf16[2,4,96,2048]{3,2,1,0:T(8,128)(2,1)S(1)}, bf16[2,4,96,2048]{3,2,1,0:T(8,128)(2,1)}, u32[]{:S(2)}) copy-start(bf16[2,4,96,2048]{3,2,1,0:T(8,128)(2,1)} %get-tuple-element.18) | copy-start | bytes 9437188
  80.6 3.5 %copy-start.7 = (bf16[8,256,512]{2,1,0:T(8,128)(2,1)S(1)}, bf16[8,256,512]{2,1,0:T(8,128)(2,1)}, u32[]{:S(2)}) copy-start(bf16[8,256,512]{2,1,0:T(8,128)(2,1)} %get-tuple-element.17) | copy-start | bytes 6291460
  89.2 3.2 %copy-start.6 = (bf16[8,256,512]{2,1,0:T(8,128)(2,1)S(1)}, bf16[8,256,512]{2,1,0:T(8,128)(2,1)}, u32[]{:S(2)}) copy-start(bf16[8,256,512]{2,1,0:T(8,128)(2,1)} %get-tuple-element.16) | copy-start | bytes 6291460
  180.0 1.7 copy-start
  181.7 1.6 copy-start.1
  183.3 1.1 copy-start.3
  183.3 1.9 %copy-start.2 = (bf16[96,2048]{1,0:T(8,128)(2,1)S(1)}, bf16[96,2048]{1,0:T(8,128)(2,1)}, u32[]{:S(2)}) copy-start(bf16[96,2048]{1,0:T(8,128)(2,1)} %get-tuple-element.37) | copy-start | bytes 1179652
